TPU v7x, 32 devices: a whole 2x2x4 slice. The times are simulated.
32 devices in a mesh: grp: 2 (over y), sp: 4 (over z), tp: 4 (over x, core).
Axes of the slice: x: 2, y: 2, z: 4, core: 2. Of those that a mesh axis runs over, the one named last changes fastest.
Arguments:
- prompt: bfloat16 [8, 6144, 2048], P('grp', 'sp'), parts along dimension 0, may hold values from -6 to 6
- w_key: bfloat16 [2048, 2048], P('sp', 'tp'), may hold values from -0.125 to 0.125
- w_value: bfloat16 [2048, 2048], P('sp', 'tp'), may hold values from -0.125 to 0.125
- query_new: bfloat16 [8, 2048], P('grp', 'tp'), parts along dimension 0, may hold values from -150 to 150
- key_new: bfloat16 [8, 2048], P('grp', 'tp'), parts along dimension 0, may hold values from -15 to 15
- value_new: bfloat16 [8, 2048], P('grp', 'tp'), parts along dimension 0, may hold values from -6 to 6
- mix_lambda: float32 [16], P('tp'), may hold values from 0.3 to 0.8
- head_gain: float32 [128], replicated, may hold values from 0.1 to 1.9
Outputs:
- key_cache: bfloat16 [8, 4, 1536, 2048], P(('grp', 'sp'), None, None, 'tp'), parts along dimension 0
- value_cache: bfloat16 [8, 4, 1536, 2048], P(('grp', 'sp'), None, None, 'tp'), parts along dimension 0
- first_read: bfloat16 [8, 2048], P('grp', 'tp'), parts along dimension 0
There are 2 independent parts, one for each index of `grp`. A program takes and returns all parts, laid end to end along the dimension named above; an argument that names none is the same for every part. Nothing has to cross between parts.
All inputs are finite; a program needn't handle non-finite values.
Results may differ from a plain program's by a relative error of at most 0.0065.
The roundings to bfloat16 on the way count: a program that leaves them out, or rounds other values in their place, can miss the bound.
Values may be sent and summed in bfloat16 or wider, within the bound.
A program may use at most 128 MiB of HBM per device.

v0:
```python
import jax
import jax.numpy as jnp
from jax import lax
from jax.sharding import PartitionSpec as P

HALF = 64
VDIM = 128


def combined_all(part, axis, combine):
    gathered = jax.tree.map(lambda a: lax.all_gather(a, axis), part)

    def take(source):
        return jax.tree.map(lambda a: lax.dynamic_index_in_dim(a, source, 0, False), gathered)

    return lax.fori_loop(
        1, lax.axis_size(axis), lambda source, state: combine(state, take(source)), take(0)
    )


def project(rows, w_key, w_value):
    keys = jnp.dot(
        rows, lax.all_gather(w_key, "sp", axis=0, tiled=True), preferred_element_type=jnp.float32
    )
    values = jnp.dot(
        rows, lax.all_gather(w_value, "sp", axis=0, tiled=True), preferred_element_type=jnp.float32
    )
    return (keys.astype(jnp.bfloat16), values.astype(jnp.bfloat16))


def score_maps(query, keys):
    count, span = (keys.shape[0], keys.shape[1])
    heads = query.shape[1] // (2 * HALF)
    q_parts = query.reshape(count, heads, 2, HALF)
    k_parts = keys.reshape(count, span, heads, 2, HALF)
    return jnp.einsum(
        "shmc,slhmc->shml", q_parts, k_parts, preferred_element_type=jnp.float32
    ) * HALF ** (-0.5)


def own_scores(query, fresh_key):
    count = query.shape[0]
    heads = query.shape[1] // (2 * HALF)
    q_parts = query.astype(jnp.float32).reshape(count, heads, 2, HALF)
    k_parts = fresh_key.astype(jnp.float32).reshape(count, heads, 2, HALF)
    return jnp.sum(q_parts * k_parts, axis=-1) * HALF ** (-0.5)


def finish(reads, head_gain):
    mean = jnp.mean(reads * reads, axis=-1, keepdims=True)
    normed = reads * lax.rsqrt(mean + 1e-06) * head_gain
    return normed.reshape(reads.shape[0], -1).astype(jnp.bfloat16)


def join_totals(first, second):
    top = jnp.maximum(first[0], second[0])
    return (top, first[1] * jnp.exp(first[0] - top) + second[1] * jnp.exp(second[0] - top))


def placed(part_rows, prompts, first, fill):
    base = jnp.full((prompts,) + part_rows.shape[1:], fill, jnp.float32)
    return lax.dynamic_update_slice_in_dim(base, part_rows, first, 0)


def cache_read(query_new, key_new, value_new, keys, values, mix_lambda, head_gain, first):
    count, span = (keys.shape[0], keys.shape[1])
    prompts = query_new.shape[0]
    heads = mix_lambda.shape[0]
    query = lax.dynamic_slice_in_dim(query_new, first, count, 0)
    scores = score_maps(query, keys)
    fresh_all = own_scores(query_new, key_new)
    fresh = lax.dynamic_slice_in_dim(fresh_all, first, count, 0)
    local_top = jnp.maximum(jnp.max(scores, axis=-1), fresh)
    local_total = jnp.sum(jnp.exp(scores - local_top[..., None]), axis=-1)
    top_all, cache_total = combined_all(
        (placed(local_top, prompts, first, -1e30), placed(local_total, prompts, first, 0.0)),
        "sp",
        join_totals,
    )
    own = jnp.exp(fresh_all - top_all)
    total_all = cache_total + own
    top = lax.dynamic_slice_in_dim(top_all, first, count, 0)
    total = lax.dynamic_slice_in_dim(total_all, first, count, 0)
    probs = jnp.exp(scores - top[..., None]) / total[..., None]
    mixed = (probs[:, :, 0] - mix_lambda[None, :, None] * probs[:, :, 1]).astype(jnp.bfloat16)
    value_parts = values.reshape(count, span, heads, VDIM)
    partial_value = jnp.einsum(
        "shl,slhv->shv", mixed, value_parts, preferred_element_type=jnp.float32
    )
    reads = lax.psum(placed(partial_value, prompts, first, 0.0), "sp")
    own_prob = own / total_all
    own_mixed = (own_prob[:, :, 0] - mix_lambda[None, :] * own_prob[:, :, 1]).astype(jnp.bfloat16)
    reads = reads + own_mixed.astype(jnp.float32)[..., None] * value_new.astype(
        jnp.float32
    ).reshape(prompts, heads, VDIM)
    return finish(reads, head_gain)


def block_read(
    query_new, key_new, value_new, key_cache, value_cache, mix_lambda, head_gain, spread
):
    blocks, sub = (key_cache.shape[1], key_cache.shape[2])
    first = lax.axis_index("sp") // spread
    keys = key_cache.reshape(1, blocks * sub, -1)
    values = value_cache.reshape(1, blocks * sub, -1)
    return cache_read(query_new, key_new, value_new, keys, values, mix_lambda, head_gain, first)


def body(prompt, w_key, w_value, query_new, key_new, value_new, mix_lambda, head_gain):
    count, piece, width = prompt.shape
    spread = lax.axis_size("sp") // count
    sub = piece // spread
    keys, values = project(prompt.reshape(count * piece, width), w_key, w_value)
    key_blocks = keys.reshape(count * spread, 1, sub, -1)
    value_blocks = values.reshape(count * spread, 1, sub, -1)
    key_cache, value_cache = (
        lax.all_to_all(key_blocks, "sp", split_axis=0, concat_axis=1, tiled=True),
        lax.all_to_all(value_blocks, "sp", split_axis=0, concat_axis=1, tiled=True),
    )
    first_read = block_read(
        query_new, key_new, value_new, key_cache, value_cache, mix_lambda, head_gain, spread
    )
    return (key_cache, value_cache, first_read)


def solution(mesh):
    placed = (
        P("grp", "sp", None),
        P("sp", "tp"),
        P("sp", "tp"),
        P("grp", "tp"),
        P("grp", "tp"),
        P("grp", "tp"),
        P("tp"),
        P(),
    )
    return jax.shard_map(
        body,
        mesh=mesh,
        in_specs=placed,
        out_specs=(
            P(("grp", "sp"), None, None, "tp"),
            P(("grp", "sp"), None, None, "tp"),
            P("grp", "tp"),
        ),
        check_vma=False,
    )
```

profile of v0, /device:TPU:0, one launch (start us, length us, event | category | flops | bytes accessed | tf_op | source)
XLA Modules:
  0.0 461.9 jit_solution(8935181542951805076)
XLA Ops:
  7.2 0.7 all-gather.3.cloned.1.call-update
  7.9 50.1 %all-gather.3.cloned.1.call-done = bf16[2048,512]{1,0:T(8,128)(2,1)} async-done(((bf16[512,512]{1,0:T(8,128)(2,1)}), bf16[2048,512]{1,0:T(8,128)(2,1)}) %all-gather.3.cloned.1.call-update) | async-done | bytes 2097168 | tf_op jit(solution)/shard_map/all_gather | solution.py:23
  58.0 20.3 %convolution_convert_fusion.1 = bf16[6144,512]{1,0:T(8,128)(2,1)} fusion(bf16[6144,2048]{1,0:T(8,128)(2,1)} %bitcast.91, bf16[2048,512]{1,0:T(8,128)(2,1)} %all-gather.3.cloned.1.call-done), kind=kOutput, calls=%fused_computation.6 | convolution fusion | flops 12888047616 | bytes 33554432 | tf_op jit(solution)/shard_map/dot_general | solution.py:22
  78.2 5.2 %all-to-all-start = ((bf16[4,1,1536,512]{3,2,1,0:T(8,128)(2,1)}), bf16[4,1,1536,512]{3,2,1,0:T(8,128)(2,1)}, u32[]{:S(2)}, u32[]{:S(2)}) async-start(bf16[4,1,1536,512]{3,2,1,0:T(8,128)(2,1)} %bitcast.82), calls=%async_computation | async-start | bytes 12582912 | tf_op jit(solution)/shard_map/all_to_all | solution.py:117
  83.5 0.2 all-gather.5.cloned.1.call-start
  83.7 0.5 all-gather.5.cloned.1.call-update
  84.2 88.2 %all-gather.5.cloned.1.call-done = bf16[2048,512]{1,0:T(8,128)(2,1)} async-done(((bf16[512,512]{1,0:T(8,128)(2,1)}), bf16[2048,512]{1,0:T(8,128)(2,1)}) %all-gather.5.cloned.1.call-update) | async-done | bytes 2097168 | tf_op jit(solution)/shard_map/all_gather | solution.py:26
  172.4 20.3 %convolution_convert_fusion = bf16[6144,512]{1,0:T(8,128)(2,1)} fusion(bf16[6144,2048]{1,0:T(8,128)(2,1)} %bitcast.92, bf16[2048,512]{1,0:T(8,128)(2,1)} %all-gather.5.cloned.1.call-done), kind=kOutput, calls=%fused_computation.5 | convolution fusion | flops 12888047616 | bytes 33554432 | tf_op jit(solution)/shard_map/dot_general | solution.py:25
  192.7 62.8 %all-to-all-done = bf16[4,1,1536,512]{3,2,1,0:T(8,128)(2,1)} async-done(((bf16[4,1,1536,512]{3,2,1,0:T(8,128)(2,1)}), bf16[4,1,1536,512]{3,2,1,0:T(8,128)(2,1)}, u32[]{:S(2)}, u32[]{:S(2)}) %all-to-all-start) | async-done | bytes 6291488 | tf_op jit(solution)/shard_map/all_to_all | solution.py:117
  255.4 5.4 %all-to-all-start.1 = ((bf16[4,1,1536,512]{3,2,1,0:T(8,128)(2,1)}), bf16[4,1,1536,512]{3,2,1,0:T(8,128)(2,1)}, u32[]{:S(2)}, u32[]{:S(2)}) async-start(bf16[4,1,1536,512]{3,2,1,0:T(8,128)(2,1)} %bitcast.81), calls=%async_computation.1 | async-start | bytes 12582912 | tf_op jit(solution)/shard_map/all_to_all | solution.py:118
  261.1 0.1 reduce_sum.27
  261.2 11.4 %copy.60 = bf16[4,1,1536,512]{2,0,3,1:T(4,128)(2,1)} copy(bf16[4,1,1536,512]{3,2,1,0:T(8,128)(2,1)} %all-to-all-done) | data formatting | bytes 12582912 | tf_op jit(solution)/shard_map/all_to_all | solution.py:117
  272.5 12.6 %reshape.109 = bf16[6144,4,2,64]{0,3,2,1:T(8,128)(2,1)} reshape(bf16[4,1,1536,512]{2,0,3,1:T(4,128)(2,1)} %copy.60) | data formatting | bytes 12582912 | tf_op jit(solution)/shard_map/reshape.7
  285.2 3.7 fusion.15
  288.9 0.2 fusion.4
  289.1 0.1 copy.61
  289.2 0.1 copy.64
  289.4 0.3 exponential_reduce_fusion
  289.8 114.1 %all_gather.23 = f32[4,4,4,2]{2,1,3,0:T(4,128)S(1)} all-gather(f32[1,4,4,2]{2,1,3,0:T(4,128)S(1)} %dynamic_update_slice.12), channel_id=1, replica_groups=mesh['grp'=2,'sp'=4,'tp'=4] {'sp'}, dimensions={0}, use_global_device_ids=true | all-gather | bytes 640 | tf_op jit(solution)/shard_map/all_gather | solution.py:11
  403.9 13.2 %all_gather.21 = f32[4,4,4,2]{2,1,3,0:T(4,128)S(1)} all-gather(f32[1,4,4,2]{2,1,3,0:T(4,128)S(1)} %dynamic_update_slice.11), channel_id=1, replica_groups=mesh['grp'=2,'sp'=4,'tp'=4] {'sp'}, dimensions={0}, use_global_device_ids=true | all-gather | bytes 640 | tf_op jit(solution)/shard_map/all_gather | solution.py:11
  417.1 0.1 while.17
  417.2 0.1 copy.66
  417.3 0.1 copy.67
  417.6 0.2 divide_bitcast_fusion
  417.9 9.7 %reshape.110 = bf16[6144,4,128]{2,1,0:T(4,128)(2,1)} reshape(bf16[4,1,1536,512]{3,2,1,0:T(8,128)(2,1)} %all-to-all-done.1) | data formatting | bytes 12582912 | tf_op jit(solution)/shard_map/reshape.31
  427.6 3.8 fusion.2
  431.4 10.9 %psum.7 = f32[4,4,128]{2,1,0:T(4,128)S(1)} all-reduce(f32[4,4,128]{2,1,0:T(4,128)S(1)} %constant_dynamic-update-slice_fusion), channel_id=1, replica_groups=mesh['grp'=2,'sp'=4,'tp'=4] {'sp'}, use_global_device_ids=true, to_apply=%region_5.6 | all-reduce | flops 2048 | bytes 16384 | tf_op jit(solution)/shard_map/psum | solution.py:90
  442.3 0.2 convert_reduce_fusion
  442.4 0.2 multiply_reduce_fusion
  442.7 0.6 copy.89
  443.3 5.9 %copy.104 = bf16[1,4,1536,512]{3,2,1,0:T(8,128)(2,1)} copy(bf16[1,4,1536,512]{3,2,1,0:T(8,128)(2,1)} %bitcast.5) | data formatting | bytes 12582912
  449.2 5.9 %copy.105 = bf16[1,4,1536,512]{3,2,1,0:T(8,128)(2,1)} copy(bf16[1,4,1536,512]{3,2,1,0:T(8,128)(2,1)} %bitcast.8) | data formatting | bytes 12582912
  (38 shorter events, 0.9 us)
Async XLA Ops:
  7.2 50.8 %all-gather.3.cloned.1.call-start = ((), (), s32[]{:S(2)}) async-start(), calls=%async_computation.2 | async-start | bytes 2621440 | tf_op jit(solution)/shard_map/all_gather | solution.py:23
  78.2 177.2 %all-to-all-start = ((bf16[4,1,1536,512]{3,2,1,0:T(8,128)(2,1)}), bf16[4,1,1536,512]{3,2,1,0:T(8,128)(2,1)}, u32[]{:S(2)}, u32[]{:S(2)}) async-start(bf16[4,1,1536,512]{3,2,1,0:T(8,128)(2,1)} %bitcast.82), calls=%async_computation | async-start | bytes 12582912 | tf_op jit(solution)/shard_map/all_to_all | solution.py:117
  83.5 88.9 %all-gather.5.cloned.1.call-start = ((), (), s32[]{:S(2)}) async-start(), calls=%async_computation.3 | async-start | bytes 2621440 | tf_op jit(solution)/shard_map/all_gather | solution.py:26
  255.4 5.4 %copy-start = (bf16[4,512]{1,0:T(4,128)(2,1)S(1)}, bf16[4,512]{1,0:T(4,128)(2,1)}, u32[]{:S(2)}) copy-start(bf16[4,512]{1,0:T(4,128)(2,1)} %param.13) | copy-start | bytes 12292
  255.4 5.5 %copy-start.2 = (bf16[4,512]{1,0:T(4,128)(2,1)S(1)}, bf16[4,512]{1,0:T(4,128)(2,1)}, u32[]{:S(2)}) copy-start(bf16[4,512]{1,0:T(4,128)(2,1)} %param.14) | copy-start | bytes 12292
  255.4 5.6 %copy-start.1 = (bf16[4,512]{1,0:T(4,128)(2,1)S(1)}, bf16[4,512]{1,0:T(4,128)(2,1)}, u32[]{:S(2)}) copy-start(bf16[4,512]{1,0:T(4,128)(2,1)} %param.15) | copy-start | bytes 12292
  255.4 162.4 %all-to-all-start.1 = ((bf16[4,1,1536,512]{3,2,1,0:T(8,128)(2,1)}), bf16[4,1,1536,512]{3,2,1,0:T(8,128)(2,1)}, u32[]{:S(2)}, u32[]{:S(2)}) async-start(bf16[4,1,1536,512]{3,2,1,0:T(8,128)(2,1)} %bitcast.81), calls=%async_computation.1 | async-start | bytes 12582912 | tf_op jit(solution)/shard_map/all_to_all | solution.py:118
  285.2 132.6 %copy-start.3 = (f32[4]{0:T(128)S(1)}, f32[4]{0:T(128)}, u32[]{:S(2)}) copy-start(f32[4]{0:T(128)} %param.16) | copy-start | bytes 52
  427.6 15.0 %copy-start.4 = (f32[128]{0:T(128)S(1)}, f32[128]{0:T(128)}, u32[]{:S(2)}) copy-start(f32[128]{0:T(128)} %param.17) | copy-start | bytes 1540
Sparse Core Ops, SparseCore 0:
  9.5 48.3 all-gather.2
  85.8 86.5 all-gather.4
where the time goes:
time: 463 us; the launch traced here: 462 us
  waiting for transfers between devices  202 us (44%)
  blocking collectives  138 us (30%)
  matrix products  48 us (10%)
  local copies, waits for them, and re-layouts  47 us (10%)
  between operations  14.2 us (3%)
  starting transfers between devices  10.9 us (2%)
    all_gather x2, blocking collectives, combined_all(): gathered = jax.tree.map(lambda a: lax.all_gather(a, axis), part)  127 us
    all_gather x1, waiting for transfers between devices, project(): lax.all_gather(w_value, 'sp', axis=0, tiled=True)  88.2 us
    all_to_all x1, waiting for transfers between devices, body(): lax.all_to_all(key_blocks, 'sp', split_axis=0, concat_axis=1, tiled=True)  62.8 us
    all_gather x1, waiting for transfers between devices, project(): lax.all_gather(w_key, 'sp', axis=0, tiled=True)  50.1 us
    another operation x3, local copies, waits for them, and re-layouts  22.4 us
    dot_general x1, matrix products, project(): jnp.dot(rows, lax.all_gather(w_value, 'sp', axis=0, tiled=True), preferre...  20.3 us
    dot_general x1, matrix products, project(): jnp.dot(rows, lax.all_gather(w_key, 'sp', axis=0, tiled=True), preferred_...  20.3 us
    unnamed x13, local copies, waits for them, and re-layouts  12.4 us
  transfers between devices with their start and end apart: 4, of which 3 were waited for; matrix products, arithmetic and copies ran while one was open for 11% of the time, Pallas kernels for 0%

commit v1 on v0

--- a/solution.py
+++ b/solution.py
@@ -1,10 +1,18 @@
+import functools
+
 import jax
 import jax.numpy as jnp
 from jax import lax
+from jax.experimental import pallas as pl
+from jax.experimental.pallas import tpu as pltpu
 from jax.sharding import PartitionSpec as P
 
 HALF = 64
 VDIM = 128
+MESH = pl.DeviceIdType.MESH
+CHUNKS = 6
+LAG_X = 1
+LAG_C = 2
 
 
 def combined_all(part, axis, combine):
@@ -123,6 +131,403 @@
     return (key_cache, value_cache, first_read)
 
 
+def gather_kernel(
+    sizes, prompt, w_key, w_value, keys, values,
+    rows_in, weights, k_buf, v_buf,
+    z_send, z_recv, x_send, x_recv, d_send, d_recv, e_send, e_recv,
+    wr_send, wr_recv, wl_send, wl_recv, wy_send, wy_recv, local, out_sem,
+):
+    n, chunks, tile, quarter = sizes
+    me = lax.axis_index("sp")
+    tp = lax.axis_index("tp")
+    grp = lax.axis_index("grp")
+    across = lax.rem(tp + 2, 4)
+    sibling = tp + 1 - 2 * lax.rem(tp, 2)
+    far = lax.rem(sibling + 2, 4)
+    depth, cols = w_key.shape
+    half = depth // 2
+    mats = (w_key, w_value)
+
+    def rows(j, q):
+        return pl.ds(pl.multiple_of(j * tile + q * quarter, quarter), quarter)
+
+    barrier = pltpu.get_barrier_semaphore()
+    for step in range(1, n):
+        pl.semaphore_signal(
+            barrier, inc=1, device_id={"sp": lax.rem(me + step, n)}, device_id_type=MESH
+        )
+    pl.semaphore_signal(barrier, inc=1, device_id={"tp": across}, device_id_type=MESH)
+    pl.semaphore_signal(barrier, inc=1, device_id={"tp": sibling}, device_id_type=MESH)
+    pl.semaphore_signal(barrier, inc=1, device_id={"grp": 1 - grp}, device_id_type=MESH)
+    pl.semaphore_wait(barrier, n + 2)
+
+    def w_slot(src, m, g):
+        return weights.at[pl.ds(pl.multiple_of(src * depth + g * half, half), half),
+                          pl.ds(m * cols, cols)]
+
+    def w_hop(src, m, to, send, recv, own):
+        origin = mats[m].at[pl.ds(pl.multiple_of(grp * half, half), half)] if own else w_slot(src, m, grp)
+        return pltpu.make_async_remote_copy(
+            src_ref=origin, dst_ref=w_slot(src, m, grp),
+            send_sem=send.at[src * 2 + m], recv_sem=recv.at[src * 2 + m],
+            device_id={"sp": to}, device_id_type=MESH,
+        )
+
+    def w_side(src, m, g):
+        return pltpu.make_async_remote_copy(
+            src_ref=w_slot(src, m, g), dst_ref=w_slot(src, m, g),
+            send_sem=wy_send.at[src * 2 + m], recv_sem=wy_recv.at[src * 2 + m],
+            device_id={"grp": 1 - grp}, device_id_type=MESH,
+        )
+
+    def z_copy(src, dst, j):
+        return pltpu.make_async_remote_copy(
+            src_ref=prompt.at[dst, rows(j, tp)], dst_ref=rows_in.at[src, rows(j, tp)],
+            send_sem=z_send.at[dst * chunks + j], recv_sem=z_recv.at[src * chunks + j],
+            device_id={"sp": dst}, device_id_type=MESH,
+        )
+
+    def side_copy(src, j, q, to, send, recv):
+        return pltpu.make_async_remote_copy(
+            src_ref=rows_in.at[src, rows(j, q)], dst_ref=rows_in.at[src, rows(j, q)],
+            send_sem=send.at[src * chunks + j], recv_sem=recv.at[src * chunks + j],
+            device_id={"tp": to}, device_id_type=MESH,
+        )
+
+    def right_sends():
+        def send(i, carry):
+            z_copy(me, me + 1 + i // chunks, lax.rem(i, chunks)).start()
+            return carry
+        lax.fori_loop(0, (n - 1 - me) * chunks, send, 0)
+
+    def left_sends():
+        def send(i, carry):
+            z_copy(me, me - 1 - i // chunks, lax.rem(i, chunks)).start()
+            return carry
+        lax.fori_loop(0, me * chunks, send, 0)
+
+    for m in range(2):
+        @pl.when(me + 1 < n)
+        def _():
+            w_hop(me, m, me + 1, wr_send, wr_recv, True).start()
+
+        @pl.when(me > 0)
+        def _():
+            w_hop(me, m, me - 1, wl_send, wl_recv, True).start()
+
+    own_w = [
+        pltpu.make_async_copy(
+            mats[m],
+            weights.at[pl.ds(pl.multiple_of(me * depth, depth), depth), pl.ds(m * cols, cols)],
+            local.at[m],
+        )
+        for m in range(2)
+    ]
+    own_rows = pltpu.make_async_copy(prompt.at[me], rows_in.at[me], local.at[2])
+    for copy in own_w:
+        copy.start()
+    own_rows.start()
+
+    @pl.when(me == 0)
+    def _():
+        right_sends()
+
+    @pl.when(me == n - 1)
+    def _():
+        left_sends()
+
+    for d in range(1, n):
+        @pl.when(me - d >= 0)
+        def _():
+            for m in range(2):
+                w_hop(me - d, m, me, wr_send, wr_recv, False).wait_recv()
+
+                @pl.when(me + 1 < n)
+                def _():
+                    w_hop(me - d, m, me + 1, wr_send, wr_recv, False).start()
+
+                w_side(me - d, m, grp).start()
+
+        @pl.when(me + d < n)
+        def _():
+            for m in range(2):
+                w_hop(me + d, m, me, wl_send, wl_recv, False).wait_recv()
+
+                @pl.when(me > 0)
+                def _():
+                    w_hop(me + d, m, me - 1, wl_send, wl_recv, False).start()
+
+                w_side(me + d, m, grp).start()
+
+        @pl.when(me == d)
+        def _():
+            right_sends()
+
+        @pl.when(n - 1 - me == d)
+        def _():
+            left_sends()
+
+    for step in range(1, n):
+        src = lax.rem(me + step, n)
+        for m in range(2):
+            w_side(src, m, 1 - grp).wait_recv()
+    for copy in own_w:
+        copy.wait()
+    own_rows.wait()
+
+    def out_copies(slot, src, j):
+        where = pl.ds(pl.multiple_of(j * tile, tile), tile)
+        return (
+            pltpu.make_async_copy(k_buf.at[slot], keys.at[src, where], out_sem.at[slot]),
+            pltpu.make_async_copy(v_buf.at[slot], values.at[src, where], out_sem.at[slot + 2]),
+        )
+
+    def compute(slot, busy, src, j):
+        block = rows_in[src, pl.ds(pl.multiple_of(j * tile, tile), tile), :]
+        both = jnp.dot(block, weights[...], preferred_element_type=jnp.float32)
+
+        @pl.when(busy)
+        def _():
+            for copy in out_copies(slot, src, j):
+                copy.wait()
+
+        k_buf[slot] = both[:, :cols].astype(jnp.bfloat16)
+        v_buf[slot] = both[:, cols:].astype(jnp.bfloat16)
+        for copy in out_copies(slot, src, j):
+            copy.start()
+
+    inner = jnp.minimum(me, n - 1 - me)
+
+    def order(k):
+        pairs = 2 * inner * chunks
+        r = lax.rem(k, 2 * chunks)
+        two = me + (k // (2 * chunks) + 1) * (1 - 2 * lax.rem(r, 2))
+        s = k - pairs
+        d = inner + 1 + s // chunks
+        one = jnp.where(me > n - 1 - me, me - d, me + d)
+        both = k < pairs
+        return jnp.where(both, two, one), jnp.where(both, r // 2, lax.rem(s, chunks))
+
+    total = (n - 1) * chunks
+
+    def step(k, carry):
+        @pl.when(k < total)
+        def _():
+            src, j = order(k)
+            z_copy(src, me, j).wait_recv()
+            side_copy(src, j, tp, across, x_send, x_recv).start()
+            side_copy(src, j, tp, sibling, d_send, d_recv).start()
+
+        @pl.when((k >= LAG_X) & (k < total + LAG_X))
+        def _():
+            src, j = order(k - LAG_X)
+            side_copy(src, j, across, across, x_send, x_recv).wait_recv()
+            side_copy(src, j, across, sibling, e_send, e_recv).start()
+
+        @pl.when(k < chunks)
+        def _():
+            compute(0, k > 0, me, k)
+
+        @pl.when(k >= LAG_C)
+        def _():
+            src, j = order(k - LAG_C)
+            side_copy(src, j, sibling, sibling, d_send, d_recv).wait_recv()
+            side_copy(src, j, far, sibling, e_send, e_recv).wait_recv()
+            compute(1, k > LAG_C, src, j)
+
+        return carry
+
+    lax.fori_loop(0, total + LAG_C, step, 0)
+
+    for slot in range(2):
+        for copy in out_copies(slot, me, 0):
+            copy.wait()
+
+    def drain(k, carry):
+        src, j = order(k)
+        z_copy(me, src, j).wait_send()
+        side_copy(src, j, tp, across, x_send, x_recv).wait_send()
+        side_copy(src, j, tp, sibling, d_send, d_recv).wait_send()
+        side_copy(src, j, across, sibling, e_send, e_recv).wait_send()
+        return carry
+
+    lax.fori_loop(0, total, drain, 0)
+    for step_ in range(1, n):
+        src = lax.rem(me + step_, n)
+        for m in range(2):
+            w_side(src, m, grp).wait_send()
+    for d in range(n):
+        for m in range(2):
+            @pl.when((me - d >= 0) & (me + 1 < n))
+            def _():
+                w_hop(me - d, m, me + 1, wr_send, wr_recv, False).wait_send()
+
+            @pl.when((me + d < n) & (me > 0))
+            def _():
+                w_hop(me + d, m, me - 1, wl_send, wl_recv, False).wait_send()
+
+
+def gather_project(n, prompt, w_key, w_value):
+    count, piece, width = prompt.shape
+    depth, cols = w_key.shape
+    tile = piece // CHUNKS
+    quarter = tile // 4
+    dma = pltpu.SemaphoreType.DMA
+    steps = n * CHUNKS
+    out = jax.ShapeDtypeStruct((n, piece, cols), jnp.bfloat16)
+    hbm = pl.BlockSpec(memory_space=pl.ANY)
+    return pl.pallas_call(
+        functools.partial(gather_kernel, (n, CHUNKS, tile, quarter)),
+        out_shape=(out, out),
+        in_specs=[hbm] * 3,
+        out_specs=(hbm, hbm),
+        scratch_shapes=[
+            pltpu.VMEM((n, piece, width), jnp.bfloat16),
+            pltpu.VMEM((n * depth, 2 * cols), jnp.bfloat16),
+            pltpu.VMEM((2, tile, cols), jnp.bfloat16),
+            pltpu.VMEM((2, tile, cols), jnp.bfloat16),
+        ]
+        + [dma((steps,))] * 8
+        + [dma((2 * n,))] * 6
+        + [dma((3,)), dma((4,))],
+        compiler_params=pltpu.CompilerParams(
+            collective_id=0, has_side_effects=True, vmem_limit_bytes=56 * 2**20
+        ),
+    )(prompt, w_key, w_value)
+
+
+def read_kernel(
+    pieces, query, key_new, value_new, lam, gain, keys_in, values_in, keys, values, read,
+    k_all, v_all, scores, in_sem, out_sem,
+):
+    span, cols = k_all.shape
+    tile = span // pieces
+    heads = cols // VDIM
+    me = lax.axis_index("sp")
+
+    def load(i):
+        where = pl.ds(i * tile, tile)
+        return (
+            pltpu.make_async_copy(keys_in.at[where], k_all.at[where], in_sem.at[2 * i]),
+            pltpu.make_async_copy(values_in.at[where], v_all.at[where], in_sem.at[2 * i + 1]),
+        )
+
+    def store(i):
+        where = pl.ds(i * tile, tile)
+        return (
+            pltpu.make_async_copy(k_all.at[where], keys.at[where], out_sem.at[2 * i]),
+            pltpu.make_async_copy(v_all.at[where], values.at[where], out_sem.at[2 * i + 1]),
+        )
+
+    for i in range(pieces):
+        for copy in load(i):
+            copy.start()
+
+    def mine(ref):
+        whole = ref[...].astype(jnp.float32)
+        here = lax.broadcasted_iota(jnp.int32, whole.shape, 0) == me
+        return jnp.sum(jnp.where(here, whole, 0.0), axis=0, keepdims=True)
+
+    shape = (2 * heads, cols)
+    row = lax.broadcasted_iota(jnp.int32, shape, 0)
+    group = lax.broadcasted_iota(jnp.int32, shape, 1) // HALF
+    part = jnp.where(row < heads, 2 * row, 2 * (row - heads) + 1) == group
+    q_row = mine(query)
+    q_mat = jnp.where(part, jnp.broadcast_to(q_row, shape), 0.0)
+    scale = HALF ** (-0.5)
+    fresh = jnp.sum(q_mat * mine(key_new), axis=1, keepdims=True) * scale
+    q_low = q_mat.astype(jnp.bfloat16)
+    for i in range(pieces):
+        for copy in load(i):
+            copy.wait()
+        for copy in store(i):
+            copy.start()
+        scores[:, i * tile:(i + 1) * tile] = lax.dot_general(
+            q_low, k_all[i * tile:(i + 1) * tile, :], (((1,), (1,)), ((), ())),
+            preferred_element_type=jnp.float32,
+        ) * scale
+    s = scores[...]
+    top = jnp.maximum(jnp.max(s, axis=1, keepdims=True), fresh)
+    e = jnp.exp(s - top)
+    own = jnp.exp(fresh - top)
+    total = jnp.sum(e, axis=1, keepdims=True) + own
+    w = e / total
+    own = own / total
+    mix = lam[...]
+    mixed = (w[:heads] - mix * w[heads:]).astype(jnp.bfloat16)
+    own_mixed = (own[:heads] - mix * own[heads:]).astype(jnp.bfloat16).astype(jnp.float32)
+    o = jnp.dot(mixed, v_all[...], preferred_element_type=jnp.float32)
+    o = o + own_mixed * mine(value_new)
+    for h in range(heads):
+        lanes = slice(h * VDIM, (h + 1) * VDIM)
+        one = o[h:h + 1, lanes]
+        mean = jnp.mean(one * one, axis=1, keepdims=True)
+        read[:, lanes] = (one * lax.rsqrt(mean + 1e-06) * gain[...]).astype(jnp.bfloat16)
+    for i in range(pieces):
+        for copy in store(i):
+            copy.wait()
+
+
+def read_call(query, key_new, value_new, mix_lambda, head_gain, keys, values):
+    span, cols = keys.shape
+    heads = mix_lambda.shape[0]
+    pieces = 12
+    hbm = pl.BlockSpec(memory_space=pl.ANY)
+    vmem = pl.BlockSpec(memory_space=pltpu.VMEM)
+    out = jax.ShapeDtypeStruct((span, cols), jnp.bfloat16)
+    dma = pltpu.SemaphoreType.DMA
+    return pl.pallas_call(
+        functools.partial(read_kernel, pieces),
+        out_shape=(out, out, jax.ShapeDtypeStruct((1, cols), jnp.bfloat16)),
+        in_specs=[vmem] * 5 + [hbm] * 2,
+        out_specs=(hbm, hbm, vmem),
+        scratch_shapes=[
+            pltpu.VMEM((span, cols), jnp.bfloat16),
+            pltpu.VMEM((span, cols), jnp.bfloat16),
+            pltpu.VMEM((2 * heads, span), jnp.float32),
+            dma((2 * pieces,)),
+            dma((2 * pieces,)),
+        ],
+        compiler_params=pltpu.CompilerParams(vmem_limit_bytes=40 * 2**20),
+    )(query, key_new, value_new, mix_lambda[:, None], head_gain[None, :], keys, values)
+
+
+def fast_body(prompt, w_key, w_value, query_new, key_new, value_new, mix_lambda, head_gain):
+    count, piece, width = prompt.shape
+    n = lax.axis_size("sp")
+    keys, values = gather_project(n, prompt, w_key, w_value)
+    cols = keys.shape[-1]
+    keys, values, read = read_call(
+        query_new, key_new, value_new, mix_lambda, head_gain,
+        keys.reshape(n * piece, cols), values.reshape(n * piece, cols),
+    )
+    return (
+        keys.reshape(1, n, piece, cols),
+        values.reshape(1, n, piece, cols),
+        lax.all_gather(read, "sp", axis=0, tiled=True),
+    )
+
+
+def choose(mesh):
+    def run(prompt, *rest):
+        sizes = dict(mesh.shape)
+        count, piece, width = prompt.shape
+        rows = rest[0].shape[0]
+        fits = (
+            sizes["grp"] == 2
+            and sizes["tp"] == 4
+            and sizes["sp"] == count
+            and count > 1
+            and piece % (64 * CHUNKS) == 0
+            and rows % 32 == 0
+            and (count * piece) % 1536 == 0
+            and count * piece * width * 2 <= 2**25
+        )
+        return (fast_body if fits else body)(prompt, *rest)
+
+    return run
+
+
 def solution(mesh):
     placed = (
         P("grp", "sp", None),
@@ -135,7 +540,7 @@
         P(),
     )
     return jax.shard_map(
-        body,
+        choose(mesh),
         mesh=mesh,
         in_specs=placed,
         out_specs=(

time: 463 us -> 238 us (0.51)
  Pallas kernels: 0 us -> 219 us
  waiting for transfers between devices: 202 us -> 0 us
  blocking collectives: 138 us -> 11.9 us
  matrix products: 48 us -> 0 us
  local copies, waits for them, and re-layouts: 47 us -> 6.91 us
  between operations: 14.2 us -> 0.69 us
  starting transfers between devices: 10.9 us -> 0 us
    pallas_call x0 -> x2, Pallas kernels: none -> 219 us  [the longest x1 213 us: gather_project(): pl.pallas_call(functools.partial(gather_kernel, (n, CHUNKS, tile, quarter...]
    all_gather x2 -> x0, waiting for transfers between devices: 138 us -> none  [the longest x1 88.2 us: project(): lax.all_gather(w_value, 'sp', axis=0, tiled=True)]
    all_gather x2 -> x1, blocking collectives: 127 us -> 11.9 us  [fast_body(): lax.all_gather(read, 'sp', axis=0, tiled=True)]
    all_to_all x2 -> x0, waiting for transfers between devices: 62.8 us -> none  [the longest x1 62.8 us: body(): lax.all_to_all(key_blocks, 'sp', split_axis=0, concat_axis=1, tiled=True)]
    dot_general x4 -> x0, matrix products: 48 us -> none  [the longest x1 20.3 us: project(): jnp.dot(rows, lax.all_gather(w_value, 'sp', axis=0, tiled=True), preferre...]
    another operation x3 -> x0, local copies, waits for them, and re-layouts: 22.4 us -> none
    all_to_all x1 -> x0, local copies, waits for them, and re-layouts: 11.4 us -> none  [body(): lax.all_to_all(key_blocks, 'sp', split_axis=0, concat_axis=1, tiled=True)]
    psum x1 -> x0, blocking collectives: 10.9 us -> none  [cache_read(): reads = lax.psum(placed(partial_value, prompts, first, 0.0), 'sp')]
  transfers between devices with their start and end apart: 4 -> 0, of which waited for: 3 -> 0; matrix products, arithmetic and copies ran while one was open for 11% -> 0% of each run, Pallas kernels for 0% -> 0%
where the time goes in v1:
time: 238 us
  Pallas kernels  219 us (92%)
  blocking collectives  11.9 us (5%)
  local copies, waits for them, and re-layouts  6.91 us (3%)
    pallas_call x1, Pallas kernels, gather_project(): pl.pallas_call(functools.partial(gather_kernel, (n, CHUNKS, tile, quarter...  213 us
    all_gather x1, blocking collectives, fast_body(): lax.all_gather(read, 'sp', axis=0, tiled=True)  11.9 us
    unnamed x13, local copies, waits for them, and re-layouts  6.17 us
    pallas_call x1, Pallas kernels, read_call(): pl.pallas_call(functools.partial(read_kernel, pieces), out_shape=(out, ou...  5.91 us

profile of v1, /device:TPU:0, one launch (start us, length us, event | category | flops | bytes accessed | tf_op | source)
XLA Modules:
  0.0 238.3 jit_solution(4614919962326379185)
XLA Ops:
  0.6 0.7 copy.13.lam
  1.4 0.0 copy-start.2
  1.4 0.0 copy-start.3
  1.4 0.0 copy-start.4
  1.4 0.0 copy-start.5
  1.4 212.8 %shard_map.103 = (bf16[4,1536,512]{2,1,0:T(8,128)(2,1)}, bf16[4,1536,512]{2,1,0:T(8,128)(2,1)}) custom-call(bf16[4,1536,2048]{2,1,0:T(8,128)(2,1)} %prompt.1, bf16[512,512]{1,0:T(8,128)(2,1)} %w_key.1, bf16[512,512]{1,0:T(8,128)(2,1)} %w_value.1), custom_call_target="tpu_custom_call" | custom-call | tf_op jit(solution)/shard_map/pallas_call | solution.py:379
  214.2 0.0 copy-done.2
  214.2 0.0 copy-done.3
  214.2 0.0 copy-done.4
  214.2 0.0 copy-done.5
  214.3 0.0 copy-start
  214.3 2.8 %copy-done = bf16[4,1536,512]{2,1,0:T(8,128)(2,1)S(1)} copy-done((bf16[4,1536,512]{2,1,0:T(8,128)(2,1)S(1)}, bf16[4,1536,512]{2,1,0:T(8,128)(2,1)}, u32[]{:S(2)}) %copy-start) | copy-done | bytes 6291480
  217.0 0.0 copy-start.1
  217.0 2.8 %copy-done.1 = bf16[4,1536,512]{2,1,0:T(8,128)(2,1)S(1)} copy-done((bf16[4,1536,512]{2,1,0:T(8,128)(2,1)S(1)}, bf16[4,1536,512]{2,1,0:T(8,128)(2,1)}, u32[]{:S(2)}) %copy-start.1) | copy-done | bytes 6291480
  219.8 5.9 %shard_map.104 = (bf16[6144,512]{1,0:T(8,128)(2,1)}, bf16[6144,512]{1,0:T(8,128)(2,1)}, bf16[1,512]{1,0:T(2,128)(2,1)S(1)}) custom-call(bf16[4,512]{1,0:T(4,128)(2,1)S(1)} %copy-done.2, bf16[4,512]{1,0:T(4,128)(2,1)S(1)} %copy-done.3, bf16[4,512]{1,0:T(4,128)(2,1)S(1)} %copy-done.4, f32[4,1]{1,0:T(4,128)S(1)} %copy.13.lam, f32[1,128]{1,0:T(1,128)S(1)} %bitcast.13, ...), custom_call_target="tpu_custom_call" | custom-call | tf_op jit(solution)/shard_map/pallas_call | solution.py:479
  225.7 11.9 %all-gather = bf16[4,1,512]{2,1,0:T(2,128)(2,1)S(1)} all-gather(bf16[1,1,512]{2,1,0:T(2,128)(2,1)S(1)} %bitcast.12), channel_id=1, replica_groups=mesh['grp'=2,'sp'=4,'tp'=4] {'sp'}, dimensions={0}, use_global_device_ids=true | all-gather | bytes 5120 | tf_op jit(solution)/shard_map/all_gather | solution.py:507
  237.7 0.6 copy.16
Async XLA Ops:
  1.4 212.8 %copy-start.2 = (bf16[4,512]{1,0:T(4,128)(2,1)S(1)}, bf16[4,512]{1,0:T(4,128)(2,1)}, u32[]{:S(2)}) copy-start(bf16[4,512]{1,0:T(4,128)(2,1)} %query.1) | copy-start | bytes 12292
  1.4 212.8 %copy-start.3 = (bf16[4,512]{1,0:T(4,128)(2,1)S(1)}, bf16[4,512]{1,0:T(4,128)(2,1)}, u32[]{:S(2)}) copy-start(bf16[4,512]{1,0:T(4,128)(2,1)} %key_new.1) | copy-start | bytes 12292
  1.4 212.9 %copy-start.4 = (bf16[4,512]{1,0:T(4,128)(2,1)S(1)}, bf16[4,512]{1,0:T(4,128)(2,1)}, u32[]{:S(2)}) copy-start(bf16[4,512]{1,0:T(4,128)(2,1)} %value_new.1) | copy-start | bytes 12292
  1.4 212.9 %copy-start.5 = (f32[128]{0:T(128)S(1)}, f32[128]{0:T(128)}, u32[]{:S(2)}) copy-start(f32[128]{0:T(128)} %param.15) | copy-start | bytes 1540
  214.3 2.8 %copy-start = (bf16[4,1536,512]{2,1,0:T(8,128)(2,1)S(1)}, bf16[4,1536,512]{2,1,0:T(8,128)(2,1)}, u32[]{:S(2)}) copy-start(bf16[4,1536,512]{2,1,0:T(8,128)(2,1)} %get-tuple-element.8) | copy-start | bytes 18874372
  217.0 2.8 %copy-start.1 = (bf16[4,1536,512]{2,1,0:T(8,128)(2,1)S(1)}, bf16[4,1536,512]{2,1,0:T(8,128)(2,1)}, u32[]{:S(2)}) copy-start(bf16[4,1536,512]{2,1,0:T(8,128)(2,1)} %get-tuple-element.9) | copy-start | bytes 18874372

commit v2 on v1

--- a/solution.py
+++ b/solution.py
@@ -10,9 +10,11 @@
 HALF = 64
 VDIM = 128
 MESH = pl.DeviceIdType.MESH
-CHUNKS = 6
+CHUNKS = 8
 LAG_X = 1
 LAG_C = 2
+EARLY = 2
+AHEAD = 24
 
 
 def combined_all(part, axis, combine):
@@ -133,9 +135,9 @@
 
 def gather_kernel(
     sizes, prompt, w_key, w_value, keys, values,
-    rows_in, weights, k_buf, v_buf,
+    rows_in, weights,
     z_send, z_recv, x_send, x_recv, d_send, d_recv, e_send, e_recv,
-    wr_send, wr_recv, wl_send, wl_recv, wy_send, wy_recv, local, out_sem,
+    wr_send, wr_recv, wl_send, wl_recv, wy_send, wy_recv, local,
 ):
     n, chunks, tile, quarter = sizes
     me = lax.axis_index("sp")
@@ -194,17 +196,22 @@
             device_id={"tp": to}, device_id_type=MESH,
         )
 
-    def right_sends():
-        def send(i, carry):
-            z_copy(me, me + 1 + i // chunks, lax.rem(i, chunks)).start()
-            return carry
-        lax.fori_loop(0, (n - 1 - me) * chunks, send, 0)
-
-    def left_sends():
-        def send(i, carry):
-            z_copy(me, me - 1 - i // chunks, lax.rem(i, chunks)).start()
-            return carry
-        lax.fori_loop(0, me * chunks, send, 0)
+    def right_send(i):
+        @pl.when(i < (n - 1 - me) * chunks)
+        def _():
+            c = jnp.maximum(n - 1 - me, 1)
+            z_copy(me, me + c - lax.rem(i, c), i // c).start()
+
+    def left_send(i):
+        @pl.when(i < me * chunks)
+        def _():
+            c = jnp.maximum(me, 1)
+            z_copy(me, me - c + lax.rem(i, c), i // c).start()
+
+    def both_sends(i, carry):
+        right_send(i)
+        left_send(i)
+        return carry
 
     for m in range(2):
         @pl.when(me + 1 < n)
@@ -230,11 +237,13 @@
 
     @pl.when(me == 0)
     def _():
-        right_sends()
+        for i in range(EARLY):
+            right_send(i)
 
     @pl.when(me == n - 1)
     def _():
-        left_sends()
+        for i in range(EARLY):
+            left_send(i)
 
     for d in range(1, n):
         @pl.when(me - d >= 0)
@@ -261,11 +270,15 @@
 
         @pl.when(me == d)
         def _():
-            right_sends()
+            for i in range(EARLY):
+                right_send(i)
 
         @pl.when(n - 1 - me == d)
         def _():
-            left_sends()
+            for i in range(EARLY):
+                left_send(i)
+
+    lax.fori_loop(EARLY, AHEAD, both_sends, 0)
 
     for step in range(1, n):
         src = lax.rem(me + step, n)
@@ -275,42 +288,22 @@
         copy.wait()
     own_rows.wait()
 
-    def out_copies(slot, src, j):
+    def compute(src, j):
         where = pl.ds(pl.multiple_of(j * tile, tile), tile)
-        return (
-            pltpu.make_async_copy(k_buf.at[slot], keys.at[src, where], out_sem.at[slot]),
-            pltpu.make_async_copy(v_buf.at[slot], values.at[src, where], out_sem.at[slot + 2]),
-        )
-
-    def compute(slot, busy, src, j):
-        block = rows_in[src, pl.ds(pl.multiple_of(j * tile, tile), tile), :]
-        both = jnp.dot(block, weights[...], preferred_element_type=jnp.float32)
-
-        @pl.when(busy)
-        def _():
-            for copy in out_copies(slot, src, j):
-                copy.wait()
-
-        k_buf[slot] = both[:, :cols].astype(jnp.bfloat16)
-        v_buf[slot] = both[:, cols:].astype(jnp.bfloat16)
-        for copy in out_copies(slot, src, j):
-            copy.start()
-
-    inner = jnp.minimum(me, n - 1 - me)
+        both = jnp.dot(
+            rows_in[src, where, :], weights[...], preferred_element_type=jnp.float32
+        ).astype(jnp.bfloat16)
+        keys[src, where, :] = both[:, :cols]
+        values[src, where, :] = both[:, cols:]
 
     def order(k):
-        pairs = 2 * inner * chunks
-        r = lax.rem(k, 2 * chunks)
-        two = me + (k // (2 * chunks) + 1) * (1 - 2 * lax.rem(r, 2))
-        s = k - pairs
-        d = inner + 1 + s // chunks
-        one = jnp.where(me > n - 1 - me, me - d, me + d)
-        both = k < pairs
-        return jnp.where(both, two, one), jnp.where(both, r // 2, lax.rem(s, chunks))
+        return lax.rem(me + 1 + lax.rem(k, n - 1), n), k // (n - 1)
 
     total = (n - 1) * chunks
 
     def step(k, carry):
+        both_sends(AHEAD + k, 0)
+
         @pl.when(k < total)
         def _():
             src, j = order(k)
@@ -326,22 +319,18 @@
 
         @pl.when(k < chunks)
         def _():
-            compute(0, k > 0, me, k)
+            compute(me, k)
 
         @pl.when(k >= LAG_C)
         def _():
             src, j = order(k - LAG_C)
             side_copy(src, j, sibling, sibling, d_send, d_recv).wait_recv()
             side_copy(src, j, far, sibling, e_send, e_recv).wait_recv()
-            compute(1, k > LAG_C, src, j)
+            compute(src, j)
 
         return carry
 
     lax.fori_loop(0, total + LAG_C, step, 0)
-
-    for slot in range(2):
-        for copy in out_copies(slot, me, 0):
-            copy.wait()
 
     def drain(k, carry):
         src, j = order(k)
@@ -374,54 +363,41 @@
     quarter = tile // 4
     dma = pltpu.SemaphoreType.DMA
     steps = n * CHUNKS
-    out = jax.ShapeDtypeStruct((n, piece, cols), jnp.bfloat16)
+    out = pltpu.VMEM((n, piece, cols), jnp.bfloat16)
+    vmem = pl.BlockSpec(memory_space=pltpu.VMEM)
     hbm = pl.BlockSpec(memory_space=pl.ANY)
     return pl.pallas_call(
         functools.partial(gather_kernel, (n, CHUNKS, tile, quarter)),
         out_shape=(out, out),
         in_specs=[hbm] * 3,
-        out_specs=(hbm, hbm),
+        out_specs=(vmem, vmem),
         scratch_shapes=[
             pltpu.VMEM((n, piece, width), jnp.bfloat16),
             pltpu.VMEM((n * depth, 2 * cols), jnp.bfloat16),
-            pltpu.VMEM((2, tile, cols), jnp.bfloat16),
-            pltpu.VMEM((2, tile, cols), jnp.bfloat16),
         ]
         + [dma((steps,))] * 8
         + [dma((2 * n,))] * 6
-        + [dma((3,)), dma((4,))],
+        + [dma((3,))],
         compiler_params=pltpu.CompilerParams(
-            collective_id=0, has_side_effects=True, vmem_limit_bytes=56 * 2**20
+            collective_id=0, has_side_effects=True, vmem_limit_bytes=36 * 2**20
         ),
     )(prompt, w_key, w_value)
 
 
 def read_kernel(
-    pieces, query, key_new, value_new, lam, gain, keys_in, values_in, keys, values, read,
-    k_all, v_all, scores, in_sem, out_sem,
+    pieces, query, key_new, value_new, lam, gain, k_all, v_all, keys, values, read,
+    scores, out_sem,
 ):
     span, cols = k_all.shape
     tile = span // pieces
     heads = cols // VDIM
     me = lax.axis_index("sp")
-
-    def load(i):
-        where = pl.ds(i * tile, tile)
-        return (
-            pltpu.make_async_copy(keys_in.at[where], k_all.at[where], in_sem.at[2 * i]),
-            pltpu.make_async_copy(values_in.at[where], v_all.at[where], in_sem.at[2 * i + 1]),
-        )
-
-    def store(i):
-        where = pl.ds(i * tile, tile)
-        return (
-            pltpu.make_async_copy(k_all.at[where], keys.at[where], out_sem.at[2 * i]),
-            pltpu.make_async_copy(v_all.at[where], values.at[where], out_sem.at[2 * i + 1]),
-        )
-
-    for i in range(pieces):
-        for copy in load(i):
-            copy.start()
+    stores = (
+        pltpu.make_async_copy(k_all, keys, out_sem.at[0]),
+        pltpu.make_async_copy(v_all, values, out_sem.at[1]),
+    )
+    for copy in stores:
+        copy.start()
 
     def mine(ref):
         whole = ref[...].astype(jnp.float32)
@@ -438,10 +414,6 @@
     fresh = jnp.sum(q_mat * mine(key_new), axis=1, keepdims=True) * scale
     q_low = q_mat.astype(jnp.bfloat16)
     for i in range(pieces):
-        for copy in load(i):
-            copy.wait()
-        for copy in store(i):
-            copy.start()
         scores[:, i * tile:(i + 1) * tile] = lax.dot_general(
             q_low, k_all[i * tile:(i + 1) * tile, :], (((1,), (1,)), ((), ())),
             preferred_element_type=jnp.float32,
@@ -462,10 +434,9 @@
         lanes = slice(h * VDIM, (h + 1) * VDIM)
         one = o[h:h + 1, lanes]
         mean = jnp.mean(one * one, axis=1, keepdims=True)
-        read[:, lanes] = (one * lax.rsqrt(mean + 1e-06) * gain[...]).astype(jnp.bfloat16)
-    for i in range(pieces):
-        for copy in store(i):
-            copy.wait()
+        read[:, lanes] = one * lax.rsqrt(mean + 1e-06) * gain[...]
+    for copy in stores:
+        copy.wait()
 
 
 def read_call(query, key_new, value_new, mix_lambda, head_gain, keys, values):
@@ -478,18 +449,59 @@
     dma = pltpu.SemaphoreType.DMA
     return pl.pallas_call(
         functools.partial(read_kernel, pieces),
-        out_shape=(out, out, jax.ShapeDtypeStruct((1, cols), jnp.bfloat16)),
-        in_specs=[vmem] * 5 + [hbm] * 2,
+        out_shape=(out, out, jax.ShapeDtypeStruct((1, cols), jnp.float32)),
+        in_specs=[vmem] * 7,
         out_specs=(hbm, hbm, vmem),
         scratch_shapes=[
-            pltpu.VMEM((span, cols), jnp.bfloat16),
-            pltpu.VMEM((span, cols), jnp.bfloat16),
             pltpu.VMEM((2 * heads, span), jnp.float32),
-            dma((2 * pieces,)),
-            dma((2 * pieces,)),
+            dma((2,)),
         ],
-        compiler_params=pltpu.CompilerParams(vmem_limit_bytes=40 * 2**20),
+        compiler_params=pltpu.CompilerParams(vmem_limit_bytes=32 * 2**20),
     )(query, key_new, value_new, mix_lambda[:, None], head_gain[None, :], keys, values)
+
+
+def share_kernel(n, mine, out, slots, send_sem, recv_sem):
+    me = lax.axis_index("sp")
+    barrier = pltpu.get_barrier_semaphore()
+    for step in range(1, n):
+        pl.semaphore_signal(
+            barrier, inc=1, device_id={"sp": lax.rem(me + step, n)}, device_id_type=MESH
+        )
+    pl.semaphore_wait(barrier, n - 1)
+
+    def copy(step, src):
+        return pltpu.make_async_remote_copy(
+            src_ref=mine, dst_ref=slots.at[src],
+            send_sem=send_sem.at[step], recv_sem=recv_sem.at[src],
+            device_id={"sp": lax.rem(me + step, n)}, device_id_type=MESH,
+        )
+
+    for step in range(1, n):
+        copy(step, me).start()
+    for step in range(1, n):
+        copy(step, lax.rem(me + step, n)).wait_recv()
+    row = mine[...]
+    for src in range(n):
+        out[src:src + 1, :] = jnp.where(me == src, row, slots[src]).astype(jnp.bfloat16)
+    for step in range(1, n):
+        copy(step, me).wait_send()
+
+
+def share(n, read):
+    vmem = pl.BlockSpec(memory_space=pltpu.VMEM)
+    dma = pltpu.SemaphoreType.DMA
+    return pl.pallas_call(
+        functools.partial(share_kernel, n),
+        out_shape=jax.ShapeDtypeStruct((n, read.shape[1]), jnp.bfloat16),
+        in_specs=[vmem],
+        out_specs=vmem,
+        scratch_shapes=[
+            pltpu.VMEM((n, 1, read.shape[1]), jnp.float32), dma((n,)), dma((n,)),
+        ],
+        compiler_params=pltpu.CompilerParams(
+            collective_id=1, has_side_effects=True, vmem_limit_bytes=2**20
+        ),
+    )(read)
 
 
 def fast_body(prompt, w_key, w_value, query_new, key_new, value_new, mix_lambda, head_gain):
@@ -504,7 +516,7 @@
     return (
         keys.reshape(1, n, piece, cols),
         values.reshape(1, n, piece, cols),
-        lax.all_gather(read, "sp", axis=0, tiled=True),
+        share(n, read),
     )
 
 

time: 238 us -> 207 us (0.87)
  Pallas kernels: 219 us -> 202 us
  blocking collectives: 11.9 us -> 0 us
  local copies, waits for them, and re-layouts: 6.91 us -> 3.43 us
    pallas_call x1, Pallas kernels: 213 us -> 184 us  [gather_project(): pl.pallas_call(functools.partial(gather_kernel, (n, CHUNKS, tile, quarter...]
    pallas_call x0 -> x1, Pallas kernels: none -> 13.1 us  [share(): pl.pallas_call(functools.partial(share_kernel, n), out_shape=jax.ShapeDty...]
    all_gather x1 -> x0, blocking collectives: 11.9 us -> none  [fast_body(): lax.all_gather(read, 'sp', axis=0, tiled=True)]
    unnamed x13, local copies, waits for them, and re-layouts: 6.17 us -> 2.69 us
where the time goes in v2:
time: 207 us; the launch traced here: 206 us
  Pallas kernels  202 us (98%)
  local copies, waits for them, and re-layouts  3.43 us (2%)
    pallas_call x1, Pallas kernels, gather_project(): pl.pallas_call(functools.partial(gather_kernel, (n, CHUNKS, tile, quarter...  184 us
    pallas_call x1, Pallas kernels, share(): pl.pallas_call(functools.partial(share_kernel, n), out_shape=jax.ShapeDty...  13.1 us
    pallas_call x1, Pallas kernels, read_call(): pl.pallas_call(functools.partial(read_kernel, pieces), out_shape=(out, ou...  4.8 us

profile of v2, /device:TPU:0, one launch (start us, length us, event | category | flops | bytes accessed | tf_op | source)
XLA Modules:
  0.0 206.5 jit_solution(17566697400336038822)
XLA Ops:
  0.6 0.7 copy.11.lam
  1.4 0.0 copy-start
  1.4 1.0 copy-done
  2.4 0.0 copy-start.1
  2.4 1.0 copy-done.1
  3.5 0.0 copy-start.2
  3.5 0.0 copy-start.3
  3.5 0.0 copy-start.4
  3.5 0.0 copy-start.5
  3.5 184.5 %shard_map.103 = (bf16[4,1536,512]{2,1,0:T(8,128)(2,1)S(1)}, bf16[4,1536,512]{2,1,0:T(8,128)(2,1)S(1)}) custom-call(bf16[4,1536,2048]{2,1,0:T(8,128)(2,1)} %prompt.1, bf16[512,512]{1,0:T(8,128)(2,1)S(1)} %copy-done, bf16[512,512]{1,0:T(8,128)(2,1)S(1)} %copy-done.1), custom_call_target="tpu_custom_call" | custom-call | tf_op jit(solution)/shard_map/pallas_call | solution.py:369
  188.0 0.0 copy-done.2
  188.0 0.0 copy-done.3
  188.0 0.0 copy-done.4
  188.0 0.0 copy-done.5
  188.0 4.8 %shard_map.104 = (bf16[6144,512]{1,0:T(8,128)(2,1)}, bf16[6144,512]{1,0:T(8,128)(2,1)}, f32[1,512]{1,0:T(1,128)S(1)}) custom-call(bf16[4,512]{1,0:T(4,128)(2,1)S(1)} %copy-done.2, bf16[4,512]{1,0:T(4,128)(2,1)S(1)} %copy-done.3, bf16[4,512]{1,0:T(4,128)(2,1)S(1)} %copy-done.4, f32[4,1]{1,0:T(4,128)S(1)} %copy.11.lam, f32[1,128]{1,0:T(1,128)S(1)} %bitcast.8, ...), custom_call_target="tpu_custom_call" | custom-call | tf_op jit(solution)/shard_map/pallas_call | solution.py:450
  192.8 13.1 %shard_map.105 = bf16[4,512]{1,0:T(4,128)(2,1)S(1)} custom-call(f32[1,512]{1,0:T(1,128)S(1)} %get-tuple-element.12.mine), custom_call_target="tpu_custom_call" | custom-call | tf_op jit(solution)/shard_map/pallas_call | solution.py:493
  205.9 0.6 copy.13
Async XLA Ops:
  1.4 1.0 copy-start
  2.4 1.0 copy-start.1
  3.5 184.5 %copy-start.2 = (bf16[4,512]{1,0:T(4,128)(2,1)S(1)}, bf16[4,512]{1,0:T(4,128)(2,1)}, u32[]{:S(2)}) copy-start(bf16[4,512]{1,0:T(4,128)(2,1)} %query.1) | copy-start | bytes 12292
  3.5 184.5 %copy-start.3 = (bf16[4,512]{1,0:T(4,128)(2,1)S(1)}, bf16[4,512]{1,0:T(4,128)(2,1)}, u32[]{:S(2)}) copy-start(bf16[4,512]{1,0:T(4,128)(2,1)} %key_new.1) | copy-start | bytes 12292
  3.5 184.5 %copy-start.4 = (bf16[4,512]{1,0:T(4,128)(2,1)S(1)}, bf16[4,512]{1,0:T(4,128)(2,1)}, u32[]{:S(2)}) copy-start(bf16[4,512]{1,0:T(4,128)(2,1)} %value_new.1) | copy-start | bytes 12292
  3.5 184.5 %copy-start.5 = (f32[128]{0:T(128)S(1)}, f32[128]{0:T(128)}, u32[]{:S(2)}) copy-start(f32[128]{0:T(128)} %param.15) | copy-start | bytes 1540

commit v3 on v2

--- a/solution.py
+++ b/solution.py
@@ -297,7 +297,17 @@
         values[src, where, :] = both[:, cols:]
 
     def order(k):
-        return lax.rem(me + 1 + lax.rem(k, n - 1), n), k // (n - 1)
+        pick = k * 0
+        for spot in range(n):
+            seq = []
+            for j in range(chunks):
+                for src in sorted(range(n), key=lambda a: -abs(a - spot)):
+                    if src != spot:
+                        slow = (src in (n // 2 - 1, n // 2)) and ((src < n // 2) != (spot < n // 2))
+                        seq.append((j * 2 + (3 if slow else 0), len(seq), src * chunks + j))
+            for at, (_, _, value) in enumerate(sorted(seq)):
+                pick = jnp.where((me == spot) & (k == at), value, pick)
+        return pick // chunks, lax.rem(pick, chunks)
 
     total = (n - 1) * chunks
 

time: 207 us -> 192 us (0.928)
  Pallas kernels: 202 us -> 188 us
    pallas_call x1, Pallas kernels: 184 us -> 175 us  [gather_project(): pl.pallas_call(functools.partial(gather_kernel, (n, CHUNKS, tile, quarter...]
    pallas_call x1, Pallas kernels: 13.1 us -> 8.18 us  [share(): pl.pallas_call(functools.partial(share_kernel, n), out_shape=jax.ShapeDty...]
where the time goes in v3:
time: 192 us
  Pallas kernels  188 us (98%)
  local copies, waits for them, and re-layouts  3.43 us (2%)
    pallas_call x1, Pallas kernels, gather_project(): pl.pallas_call(functools.partial(gather_kernel, (n, CHUNKS, tile, quarter...  175 us
    pallas_call x1, Pallas kernels, share(): pl.pallas_call(functools.partial(share_kernel, n), out_shape=jax.ShapeDty...  8.18 us
    pallas_call x1, Pallas kernels, read_call(): pl.pallas_call(functools.partial(read_kernel, pieces), out_shape=(out, ou...  4.8 us

profile of v3, /device:TPU:0, one launch (start us, length us, event | category | flops | bytes accessed | tf_op | source)
XLA Modules:
  0.0 191.9 jit_solution(7621364451693554776)
XLA Ops:
  0.6 0.7 copy.11.lam
  1.4 0.0 copy-start
  1.4 1.0 copy-done
  2.4 0.0 copy-start.1
  2.4 1.0 copy-done.1
  3.5 0.0 copy-start.2
  3.5 0.0 copy-start.3
  3.5 0.0 copy-start.4
  3.5 0.0 copy-start.5
  3.5 174.8 %shard_map.103 = (bf16[4,1536,512]{2,1,0:T(8,128)(2,1)S(1)}, bf16[4,1536,512]{2,1,0:T(8,128)(2,1)S(1)}) custom-call(bf16[4,1536,2048]{2,1,0:T(8,128)(2,1)} %prompt.1, bf16[512,512]{1,0:T(8,128)(2,1)S(1)} %copy-done, bf16[512,512]{1,0:T(8,128)(2,1)S(1)} %copy-done.1), custom_call_target="tpu_custom_call" | custom-call | tf_op jit(solution)/shard_map/pallas_call | solution.py:379
  178.3 0.0 copy-done.2
  178.3 0.0 copy-done.3
  178.3 0.0 copy-done.4
  178.3 0.0 copy-done.5
  178.3 4.8 %shard_map.104 = (bf16[6144,512]{1,0:T(8,128)(2,1)}, bf16[6144,512]{1,0:T(8,128)(2,1)}, f32[1,512]{1,0:T(1,128)S(1)}) custom-call(bf16[4,512]{1,0:T(4,128)(2,1)S(1)} %copy-done.2, bf16[4,512]{1,0:T(4,128)(2,1)S(1)} %copy-done.3, bf16[4,512]{1,0:T(4,128)(2,1)S(1)} %copy-done.4, f32[4,1]{1,0:T(4,128)S(1)} %copy.11.lam, f32[1,128]{1,0:T(1,128)S(1)} %bitcast.8, ...), custom_call_target="tpu_custom_call" | custom-call | tf_op jit(solution)/shard_map/pallas_call | solution.py:460
  183.1 8.2 %shard_map.105 = bf16[4,512]{1,0:T(4,128)(2,1)S(1)} custom-call(f32[1,512]{1,0:T(1,128)S(1)} %get-tuple-element.12.mine), custom_call_target="tpu_custom_call" | custom-call | tf_op jit(solution)/shard_map/pallas_call | solution.py:503
  191.3 0.6 copy.13
Async XLA Ops:
  1.4 1.0 copy-start
  2.4 1.0 copy-start.1
  3.5 174.8 %copy-start.2 = (bf16[4,512]{1,0:T(4,128)(2,1)S(1)}, bf16[4,512]{1,0:T(4,128)(2,1)}, u32[]{:S(2)}) copy-start(bf16[4,512]{1,0:T(4,128)(2,1)} %query.1) | copy-start | bytes 12292
  3.5 174.9 %copy-start.3 = (bf16[4,512]{1,0:T(4,128)(2,1)S(1)}, bf16[4,512]{1,0:T(4,128)(2,1)}, u32[]{:S(2)}) copy-start(bf16[4,512]{1,0:T(4,128)(2,1)} %key_new.1) | copy-start | bytes 12292
  3.5 174.9 %copy-start.4 = (bf16[4,512]{1,0:T(4,128)(2,1)S(1)}, bf16[4,512]{1,0:T(4,128)(2,1)}, u32[]{:S(2)}) copy-start(bf16[4,512]{1,0:T(4,128)(2,1)} %value_new.1) | copy-start | bytes 12292
  3.5 174.9 %copy-start.5 = (f32[128]{0:T(128)S(1)}, f32[128]{0:T(128)}, u32[]{:S(2)}) copy-start(f32[128]{0:T(128)} %param.15) | copy-start | bytes 1540
